TPU v7x, 32 devices: a whole 2x2x4 slice. The times are simulated.
32 devices in a mesh: sp: 4 (over z), fs: 4 (over y, x), tp: 2 (over core).
Axes of the slice: x: 2, y: 2, z: 4, core: 2. Of those that a mesh axis runs over, the one named last changes fastest.
Arguments:
- hidden_in: bfloat16 [4, 1024, 2048], P('fs', 'sp', 'tp'), may hold values from -6 to 6
- sb_query_w: bfloat16 [2048, 1024], P('fs', 'tp'), may hold values from -0.21875 to 0.21875
- sb_key_w: bfloat16 [2048, 1024], P('fs', 'tp'), may hold values from -0.21875 to 0.21875
- sb_value_w: bfloat16 [2048, 1024], P('fs', 'tp'), may hold values from -0.125 to 0.125
- sb_offset: float32 [16], P('tp'), may hold values from -16 to -6
- delta_query_w: bfloat16 [2048, 1024], P('fs', 'tp'), may hold values from -0.125 to 0.125
- delta_key_w: bfloat16 [2048, 1024], P('fs', 'tp'), may hold values from -0.125 to 0.125
- delta_value_w: bfloat16 [2048, 1024], P('fs', 'tp'), may hold values from -0.125 to 0.125
- decay_w: bfloat16 [2048, 8], P(None, 'tp'), may hold values from -0.125 to 0.125
- write_w: bfloat16 [2048, 8], P(None, 'tp'), may hold values from -0.125 to 0.125
- write_bias: float32 [8], P('tp'), may hold values from -7 to 1.5
- decay_log_scale: float32 [8], P('tp'), may hold values from -14 to -3
- decay_shift: float32 [4, 8, 1024], P('fs', 'tp', 'sp'), may hold values from -3 to 0
- head_gain: float32 [128], replicated, may hold values from 0.1 to 1.9
- sb_out_w: bfloat16 [1024, 2048], P('tp'), may hold values from -0.125 to 0.125
- delta_out_w: bfloat16 [1024, 2048], P('tp'), may hold values from -0.125 to 0.125
Outputs:
- mixed_out: bfloat16 [4, 1024, 2048], P('fs', ('sp', 'tp'))
All inputs are finite; a program needn't handle non-finite values.
Results may differ from a plain program's by a relative error of at most 0.015.
Values may be sent and summed in bfloat16 or wider, within the bound.
A program may use at most 128 MiB of HBM per device.

v0:
```python
import jax
import jax.numpy as jnp
from jax import lax
from jax.sharding import PartitionSpec as P

SB_DIM = 64
GDN_DIM = 128
BLOCK = 64


EXACT_MATMUL = lax.Precision.HIGHEST
NORM_EPS = 1e-06


def carried_in(value, axis, combine, identity):
    devices, index = (lax.axis_size(axis), lax.axis_index(axis))
    everything = jax.tree.map(
        lambda part, kind: lax.all_gather(part.astype(kind), axis),
        value,
        (jnp.bfloat16, jnp.bfloat16),
    )
    start = jax.tree.map(
        lambda part, zero: jnp.broadcast_to(jnp.asarray(zero, part.dtype), part.shape),
        value,
        identity,
    )

    def lap(k, before):
        reached = k < index
        new = combine(
            before, jax.tree.map(lambda part, own: part[k].astype(own.dtype), everything, value)
        )
        return jax.tree.map(lambda a, b: jnp.where(reached, a, b), new, before)

    return lax.fori_loop(0, devices, lap, start)


def unit_lower_inverse(strict_part):
    order_size = strict_part.shape[-1]
    powered = strict_part
    inverse = jnp.eye(order_size, dtype=strict_part.dtype) - strict_part
    for repeat_number in range(max(1, (order_size - 1).bit_length()) - 1):
        powered = jnp.einsum("...ij,...jk->...ik", powered, powered, precision=EXACT_MATMUL)
        inverse = inverse + jnp.einsum(
            "...ij,...jk->...ik", inverse, powered, precision=EXACT_MATMUL
        )
    return inverse


def to_blocks(row_data, block_span):
    blocks_count = row_data.shape[0] // block_span
    shaped = row_data.reshape((blocks_count, block_span) + row_data.shape[1:])
    return jnp.swapaxes(shaped, 1, 2)


def from_blocks(blocked):
    swapped = jnp.swapaxes(blocked, 1, 2)
    return swapped.reshape((-1,) + swapped.shape[2:])


def unit_rows(vectors):
    return vectors * lax.rsqrt(jnp.sum(vectors * vectors, axis=-1, keepdims=True) + NORM_EPS)


def delta_inputs(
    query_proj,
    key_proj,
    value_proj,
    decay_pre,
    write_pre,
    write_bias,
    decay_log_scale,
    shift_rows,
    head_count,
    head_size,
):
    query_act = jax.nn.silu(query_proj.astype(jnp.float32)).reshape(-1, head_count, head_size)
    key_act = jax.nn.silu(key_proj.astype(jnp.float32)).reshape(-1, head_count, head_size)
    value_rows = jax.nn.silu(value_proj.astype(jnp.float32)).reshape(-1, head_count, head_size)
    queries = unit_rows(query_act) * head_size ** (-0.5)
    key_rows = unit_rows(key_act)
    log_decay = -jnp.exp(decay_log_scale) * jax.nn.softplus(decay_pre) + shift_rows
    strength = jax.nn.sigmoid(write_pre + write_bias)
    return (queries, key_rows, value_rows, log_decay, strength)


def delta_prepare(queries, key_rows, value_rows, log_decay, strength):
    block_span = queries.shape[2]
    cumulative = jnp.cumsum(log_decay, axis=-1)
    row_place = lax.broadcasted_iota(jnp.int32, (block_span, block_span), 0)
    col_place = lax.broadcasted_iota(jnp.int32, (block_span, block_span), 1)
    inclusive = col_place <= row_place
    strictly = col_place < row_place
    spread = cumulative[..., :, None] - cumulative[..., None, :]
    decay_table = jnp.where(inclusive, jnp.exp(jnp.where(inclusive, spread, 0.0)), 0.0)
    keys_beta = key_rows * strength[..., None]
    lower_part = jnp.where(
        strictly,
        jnp.einsum("nhik,nhjk->nhij", keys_beta, key_rows, precision=EXACT_MATMUL) * decay_table,
        0.0,
    )
    inverse = unit_lower_inverse(lower_part)
    growth = jnp.exp(cumulative)
    state_updates = jnp.einsum(
        "nhij,nhjv->nhiv", inverse, value_rows * strength[..., None], precision=EXACT_MATMUL
    )
    erase_term = jnp.einsum(
        "nhij,nhjk->nhik", inverse, keys_beta * growth[..., None], precision=EXACT_MATMUL
    )
    inside_block = (
        jnp.einsum("nhik,nhjk->nhij", queries, key_rows, precision=EXACT_MATMUL) * decay_table
    )
    boosted_query = queries * growth[..., None]
    damped_keys = key_rows * jnp.exp(cumulative[..., -1:] - cumulative)[..., None]
    decay_per_block = jnp.exp(cumulative[..., -1])
    return (state_updates, erase_term, inside_block, boosted_query, damped_keys, decay_per_block)


def delta_step(memory_state, inputs):
    state_updates, erase_term, inside_block, boosted_query, damped_keys, decay_per_block = inputs
    fixed_values = state_updates - jnp.einsum(
        "mzq,mqc->mzc", erase_term, memory_state, precision=EXACT_MATMUL
    )
    produced_rows = jnp.einsum(
        "mzq,mqc->mzc", boosted_query, memory_state, precision=EXACT_MATMUL
    ) + jnp.einsum("efq,eqn->efn", inside_block, fixed_values, precision=EXACT_MATMUL)
    memory_state = memory_state * decay_per_block[:, None, None] + jnp.einsum(
        "wam,waz->wmz", damped_keys, fixed_values, precision=EXACT_MATMUL
    )
    return (memory_state, produced_rows)


def transition_step(carried, inputs):
    memory_state, transfer = carried
    state_updates, erase_term, inside_block, boosted_query, damped_keys, decay_per_block = inputs
    fixed_values = state_updates - jnp.einsum(
        "mzq,mqc->mzc", erase_term, memory_state, precision=EXACT_MATMUL
    )
    coupling = jnp.einsum("hik,hil->hkl", damped_keys, erase_term, precision=EXACT_MATMUL)
    memory_state = memory_state * decay_per_block[:, None, None] + jnp.einsum(
        "wam,waz->wmz", damped_keys, fixed_values, precision=EXACT_MATMUL
    )
    transfer = transfer * decay_per_block[:, None, None] - jnp.einsum(
        "hkl,hlm->hkm", coupling, transfer, precision=EXACT_MATMUL
    )
    return ((memory_state, transfer), None)


def compose(prior_blocks, following_blocks):
    joined_map = jnp.einsum(
        "hkl,hlm->hkm", following_blocks[0], prior_blocks[0], precision=EXACT_MATMUL
    )
    joined_state = (
        jnp.einsum("djo,dog->djg", following_blocks[0], prior_blocks[1], precision=EXACT_MATMUL)
        + following_blocks[1]
    )
    return (joined_map, joined_state)


def stick_block(queries, key_rows, value_rows, query_place, key_place, offsets):
    scale_factor = queries.shape[-1] ** (-0.5)
    scores = (
        jnp.einsum("qhd,khd->hqk", queries, key_rows, preferred_element_type=jnp.float32)
        * scale_factor
        + offsets[:, None, None]
    )
    visible = key_place[None, :] < query_place[:, None]
    skipped = jnp.where(visible, jax.nn.log_sigmoid(-scores), 0.0)
    beyond = lax.cumsum(skipped, axis=2, reverse=True) - skipped
    weights = jnp.where(visible, jnp.exp(jax.nn.log_sigmoid(scores) + beyond), 0.0).astype(
        jnp.bfloat16
    )
    partial_value = jnp.einsum(
        "hqk,khd->qhd", weights, value_rows, preferred_element_type=jnp.float32
    )
    return (partial_value, jnp.sum(skipped, axis=2).T)


def stick_combine(partials, totals):
    beyond = jnp.cumsum(totals[::-1], axis=0)[::-1] - totals
    return jnp.sum(partials * jnp.exp(beyond)[..., None], axis=0)


def on_device(
    hidden_in,
    sb_query_w,
    sb_key_w,
    sb_value_w,
    sb_offset,
    delta_query_w,
    delta_key_w,
    delta_value_w,
    decay_w,
    write_w,
    write_bias,
    decay_log_scale,
    decay_shift,
    head_gain,
    sb_out_w,
    delta_out_w,
):
    token_rows = hidden_in.shape[1]
    local_in = hidden_in.reshape(token_rows, hidden_in.shape[2])
    gathered = (
        lax.all_gather(sb_query_w, "fs", axis=0, tiled=True),
        lax.all_gather(sb_key_w, "fs", axis=0, tiled=True),
        lax.all_gather(sb_value_w, "fs", axis=0, tiled=True),
        lax.all_gather(delta_query_w, "fs", axis=0, tiled=True),
        lax.all_gather(delta_key_w, "fs", axis=0, tiled=True),
        lax.all_gather(delta_value_w, "fs", axis=0, tiled=True),
    )
    in_weights = tuple(gathered) + (decay_w, write_w)
    portion = lax.all_gather(local_in, "tp", axis=1, tiled=True)
    projected = tuple(
        (jnp.dot(portion, weight, preferred_element_type=jnp.float32) for weight in in_weights)
    )
    sb_heads = sb_offset.shape[0]
    delta_heads = decay_log_scale.shape[0]
    sb_query = projected[0].astype(jnp.bfloat16).reshape(token_rows, sb_heads, SB_DIM)
    sb_keys = projected[1].astype(jnp.bfloat16)
    sb_values = projected[2].astype(jnp.bfloat16)
    shift_rows = decay_shift.reshape(delta_heads, token_rows).T
    queries, key_rows, value_rows, log_decay, strength = delta_inputs(
        projected[3].astype(jnp.bfloat16),
        projected[4].astype(jnp.bfloat16),
        projected[5].astype(jnp.bfloat16),
        projected[6],
        projected[7],
        write_bias,
        decay_log_scale,
        shift_rows,
        delta_heads,
        GDN_DIM,
    )
    prepared = delta_prepare(
        to_blocks(queries, BLOCK),
        to_blocks(key_rows, BLOCK),
        to_blocks(value_rows, BLOCK),
        to_blocks(log_decay, BLOCK),
        to_blocks(strength, BLOCK),
    )
    identity_map = jnp.broadcast_to(
        jnp.eye(GDN_DIM, dtype=jnp.float32), (delta_heads, GDN_DIM, GDN_DIM)
    )
    empty_state = jnp.zeros((delta_heads, GDN_DIM, GDN_DIM), jnp.float32)
    (local_end, local_map), unused_out = lax.scan(
        transition_step, (empty_state, identity_map), prepared
    )
    own_first = lax.axis_index("sp") * token_rows
    query_place = own_first + lax.iota(jnp.int32, token_rows)
    sp_count = lax.axis_size("sp")
    slot_out = jnp.zeros((sp_count, token_rows, sb_heads, SB_DIM), jnp.float32)
    slot_total = jnp.zeros((sp_count, token_rows, sb_heads), jnp.float32)

    def absorb(slot_arrays, address_portion, value_part, shard_first):

        def active(current):
            partial_value, totals = stick_block(
                sb_query,
                address_portion.reshape(token_rows, sb_heads, SB_DIM),
                value_part.reshape(token_rows, sb_heads, SB_DIM),
                query_place,
                shard_first + lax.iota(jnp.int32, token_rows),
                sb_offset,
            )
            slot_index = shard_first // token_rows
            return (
                lax.dynamic_update_index_in_dim(current[0], partial_value, slot_index, 0),
                lax.dynamic_update_index_in_dim(current[1], totals, slot_index, 0),
            )

        def inactive(current):
            return current

        usable = jnp.logical_and(shard_first >= 0, shard_first <= own_first)
        return lax.cond(usable, active, inactive, slot_arrays)

    key_block = lax.all_gather(sb_keys, "sp", axis=0, tiled=True)
    value_block = lax.all_gather(sb_values, "sp", axis=0, tiled=True)

    def per_shard(shard_number, current):
        row_begin = shard_number * token_rows
        return absorb(
            current,
            lax.dynamic_slice_in_dim(key_block, row_begin, token_rows, 0),
            lax.dynamic_slice_in_dim(value_block, row_begin, token_rows, 0),
            row_begin,
        )

    slot_arrays = lax.fori_loop(
        0, key_block.shape[0] // token_rows, per_shard, (slot_out, slot_total)
    )
    unused_map, incoming = carried_in(
        (local_map, local_end), "sp", compose, (identity_map, empty_state)
    )
    sb_mixed = (
        stick_combine(slot_arrays[0], slot_arrays[1])
        .astype(jnp.bfloat16)
        .reshape(token_rows, sb_heads * SB_DIM)
    )
    unused_end, produced_rows = lax.scan(delta_step, incoming, prepared)
    produced_rows = from_blocks(produced_rows)
    normed = (
        produced_rows
        * lax.rsqrt(jnp.mean(produced_rows * produced_rows, axis=-1, keepdims=True) + NORM_EPS)
        * head_gain
    )
    delta_mixed = normed.astype(jnp.bfloat16).reshape(token_rows, delta_heads * GDN_DIM)
    result = lax.psum_scatter(
        (
            jnp.dot(sb_mixed, sb_out_w, preferred_element_type=jnp.float32)
            + jnp.dot(delta_mixed, delta_out_w, preferred_element_type=jnp.float32)
        ).astype(jnp.bfloat16),
        "tp",
        scatter_dimension=0,
        tiled=True,
    ).astype(jnp.float32)
    return result.astype(jnp.bfloat16).reshape(1, result.shape[0], result.shape[1])


def solution(mesh):
    return jax.shard_map(
        on_device,
        mesh=mesh,
        in_specs=(
            P("fs", "sp", "tp"),
            P("fs", "tp"),
            P("fs", "tp"),
            P("fs", "tp"),
            P("tp"),
            P("fs", "tp"),
            P("fs", "tp"),
            P("fs", "tp"),
            P(None, "tp"),
            P(None, "tp"),
            P("tp"),
            P("tp"),
            P("fs", "tp", "sp"),
            P(),
            P("tp", None),
            P("tp", None),
        ),
        out_specs=P("fs", ("sp", "tp"), None),
        check_vma=False,
    )
```

profile of v0, /device:TPU:0, one launch (start us, length us, event | category | flops | bytes accessed | tf_op | source)
XLA Modules:
  0.0 387.4 jit_solution(17021583337816945138)
XLA Ops:
  12.1 8.6 %all-gather.29.cloned.1.call-done = bf16[1,256,2048]{2,1,0:T(8,128)(2,1)} async-done(((bf16[1,256,1024]{2,1,0:T(8,128)(2,1)}), bf16[1,256,2048]{2,1,0:T(8,128)(2,1)}) %all-gather.29.cloned.1.call-update) | async-done | bytes 1048592 | tf_op jit(solution)/shard_map/all_gather | solution.py:213
  25.4 33.6 %all-gather.23.cloned.1.call-done = bf16[2048,512]{1,0:T(8,128)(2,1)} async-done(((bf16[512,512]{1,0:T(8,128)(2,1)}), bf16[2048,512]{1,0:T(8,128)(2,1)}) %all-gather.23.cloned.1.call-update) | async-done | bytes 2097168 | tf_op jit(solution)/shard_map/all_gather | solution.py:209
  58.9 3.7 fusion.116
  74.3 21.7 %all-gather.25.cloned.1.call-done = bf16[2048,512]{1,0:T(8,128)(2,1)} async-done(((bf16[512,512]{1,0:T(8,128)(2,1)}), bf16[2048,512]{1,0:T(8,128)(2,1)}) %all-gather.25.cloned.1.call-update) | async-done | bytes 2097168 | tf_op jit(solution)/shard_map/all_gather | solution.py:210
  96.0 3.5 divide_multiply_fusion.1
  99.5 2.0 reshape_reshape.3
  103.5 2.1 fusion.78
  107.1 25.7 %all-gather.27.cloned.1.call-done = bf16[2048,512]{1,0:T(8,128)(2,1)} async-done(((bf16[512,512]{1,0:T(8,128)(2,1)}), bf16[2048,512]{1,0:T(8,128)(2,1)}) %all-gather.27.cloned.1.call-update) | async-done | bytes 2097168 | tf_op jit(solution)/shard_map/all_gather | solution.py:208
  132.9 3.8 fusion.117
  140.3 2.1 reshape.155
  142.3 2.9 bitcast_multiply_fusion.1
  145.3 19.1 %while.57 = (s32[]{:T(128)}, f32[4,128,128]{2,1,0:T(8,128)S(1)}, f32[4,128,128]{2,1,0:T(8,128)S(1)}, f32[4,4]{1,0:T(4,128)S(1)}, f32[4,4,64,128]{3,2,1,0:T(8,128...) while((s32[]{:T(128)}, f32[4,128,128]{2,1,0:T(8,128)S(1)}, ...), condition=%wide.region_12.13_spmd.clone, body=%wide.region_11.12_spmd.clone.sunk | while | flops 252084224 | bytes 3279532 | solution.py:246
  165.0 16.0 %all-gather.1 = bf16[16,128,128]{2,1,0:T(8,128)(2,1)} all-gather(bf16[4,128,128]{2,1,0:T(8,128)(2,1)S(1)} %convert_element_type.96), channel_id=3, replica_groups=mesh['sp'=4,'fs'=4,'tp'=2] {'sp'}, dimensions={0}, use_global_device_ids=true | all-gather | bytes 655360 | tf_op jit(solution)/shard_map/all_gather | solution.py:18
  180.9 3.4 convolution_convert_fusion.5
  184.4 17.0 %all-gather.2 = bf16[16,128,128]{2,1,0:T(8,128)(2,1)} all-gather(bf16[4,128,128]{2,1,0:T(8,128)(2,1)S(1)} %convert_element_type.97), channel_id=4, replica_groups=mesh['sp'=4,'fs'=4,'tp'=2] {'sp'}, dimensions={0}, use_global_device_ids=true | all-gather | bytes 655360 | tf_op jit(solution)/shard_map/all_gather | solution.py:18
  201.4 3.0 convolution_multiply_fusion
  204.5 2.2 all-gather.19.cloned.1.call-done
  206.7 3.3 convolution_convert_fusion.3
  210.0 5.3 %while.58 = (s32[]{:T(128)}, f32[4,128,128]{2,1,0:T(8,128)S(1)}, s32[]{:T(128)}, bf16[4,4,128,128]{3,2,1,0:T(8,128)(2,1)}, bf16[4,4,128,128]{3,2,1,0:T(8,128)(2,1)}, /*index=5*/s32[]{:T(128)}, s32[]{:T(128)}) while((s32[]{:T(128)}, f32[4,128,128]{2,1,0:T(8,128)S(1)}, s32[]{:T(128)}, bf16[4,4,128,128]{3,2,1,0:T(8,128)(2,1)}, ...), condition=%wide.region_14.15_spmd.clone, body=%wide.region_13.14_spmd.clone.sunk | while | flops 100990976 | bytes 1575519 | solution.py:35
  215.4 23.9 %while.56 = (s32[]{:T(128)}, f32[4,128,128]{2,1,0:T(8,128)S(1)}, f32[4,4,64,128]{3,2,1,0:T(8,128)S(1)}, f32[4,4]{1,0:T(4,128)}, f32[4,4,64,128]{3,2,1,0:T(8,128)...) while((s32[]{:T(128)}, f32[4,128,128]{2,1,0:T(8,128)S(1)}, ...), condition=%wide.region_17.18_spmd, body=%wide.region_16.17_spmd.sunk | while | flops 176357376 | bytes 2493593 | solution.py:301
  240.8 2.9 all-gather.17.cloned.1.call-done
  243.7 2.6 convolution_convert_fusion.4
  247.2 26.1 %all-gather.15.cloned.1.call-done = bf16[1024,512]{1,0:T(8,128)(2,1)} async-done(((bf16[256,512]{1,0:T(8,128)(2,1)}), bf16[1024,512]{1,0:T(8,128)(2,1)}) %all-gather.15.cloned.1.call-update) | async-done | bytes 1048592 | tf_op jit(solution)/shard_map/all_gather | solution.py:278
  273.3 2.3 copy.80
  275.6 26.7 %all-gather.21.cloned.1.call-done = bf16[1024,512]{1,0:T(8,128)(2,1)} async-done(((bf16[256,512]{1,0:T(8,128)(2,1)}), bf16[1024,512]{1,0:T(8,128)(2,1)}) %all-gather.21.cloned.1.call-update) | async-done | bytes 1048592 | tf_op jit(solution)/shard_map/all_gather | solution.py:279
  302.3 2.3 copy.81
  306.8 14.7 %while.59 = (s32[]{:T(128)}, f32[4,256,8,64]{1,3,2,0:T(8,128)}, f32[4,256,8]{1,2,0:T(8,128)}, s32[]{:T(128)}, bf16[1024,512]{0,1:T(8,128)(2,1)}, /*index=5*/bf16...) while((s32[]{:T(128)}, f32[4,256,8,64]{1,3,2,0:T(8,128)}, ...), condition=%wide.region_6.7_spmd.clone.clone, body=%wide.region_0.6_spmd.clone.clone.sunk | while | flops 218698256 | bytes 25745960 | solution.py:290
  306.8 14.7 %conditional.4 = ((f32[4,256,8,64]{1,3,2,0:T(8,128)}, f32[4,256,8]{1,2,0:T(8,128)})) conditional(s32[]{:T(128)} %convert_element_type.140, (f32[4,256,8,64]{1,3,2,0:T(8,128)}, f32[4,256,8]{1,2,0:T(8,128)}) %tuple.124, (s32[]{:T(128)}, s32[]{:T(128)}, bf16[1024,512]{0,1:T(8,128)(2,1)}, bf16[256,8,64]{0,2,1:T(8,128)(2,1)}, f32[8]{0:T(128)S(1)}, ...), branch_computations={%region_1.1_spmd, %region_2.0_spmd} | conditional | flops 218698256 | bytes 25744700 | solution.py:276
  308.0 2.7 fusion.17
  310.7 5.1 %fusion.13 = f32[8,256,2,128]{1,0,3,2:T(8,128)S(1)} fusion(f32[8,256,2,128]{1,3,2,0:T(8,128)S(1)} %bitcast.258), kind=kOutput, calls=%fused_computation.18 | output fusion | flops 66584576 | bytes 4194304 | tf_op jit(solution)/shard_map/reduce-window.6
  316.7 3.0 fusion.6
  328.6 51.9 %reduce-scatter.2.cloned.1.call-done = bf16[128,2048]{1,0:T(8,128)(2,1)} async-done(((bf16[256,2048]{1,0:T(8,128)(2,1)}), bf16[128,2048]{1,0:T(8,128)(2,1)}) %reduce-scatter.2.cloned.1.call-update) | async-done | bytes 524304 | tf_op jit(solution)/shard_map/reduce_scatter | solution.py:309
  (184 shorter events, 92.5 us)
Async XLA Ops:
  6.5 318.5 %copy-start = (bf16[512,2048]{1,0:T(8,128)(2,1)S(1)}, bf16[512,2048]{1,0:T(8,128)(2,1)}, u32[]{:S(2)}) copy-start(bf16[512,2048]{1,0:T(8,128)(2,1)} %param.40) | copy-start | bytes 6291460
  6.5 4.9 %copy-start.18 = (f32[4]{0:T(128)S(1)}, f32[4]{0:T(128)}, u32[]{:S(2)}) copy-start(f32[4]{0:T(128)} %param.37) | copy-start | bytes 52
  6.5 4.9 %copy-start.17 = (f32[128]{0:T(128)S(1)}, f32[128]{0:T(128)}, u32[]{:S(2)}) copy-start(f32[128]{0:T(128)} %param.39) | copy-start | bytes 1540
  6.5 14.1 %copy-start.9 = (bf16[2048,4]{0,1:T(4,128)(2,1)S(1)}, bf16[2048,4]{0,1:T(4,128)(2,1)}, u32[]{:S(2)}) copy-start(bf16[2048,4]{0,1:T(4,128)(2,1)} %param.34) | copy-start | bytes 49156
  6.5 14.1 %copy-start.14 = (f32[1,4,256]{2,1,0:T(4,128)S(1)}, f32[1,4,256]{2,1,0:T(4,128)}, u32[]{:S(2)}) copy-start(f32[1,4,256]{2,1,0:T(4,128)} %param.38) | copy-start | bytes 12292
  6.5 14.1 %all-gather.29.cloned.1.call-start = ((), (), s32[]{:S(2)}) async-start(), calls=%async_computation.10 | async-start | bytes 1572864 | tf_op jit(solution)/shard_map/all_gather | solution.py:213
  7.3 16.3 %copy-start.10 = (bf16[2048,4]{0,1:T(4,128)(2,1)S(1)}, bf16[2048,4]{0,1:T(4,128)(2,1)}, u32[]{:S(2)}) copy-start(bf16[2048,4]{0,1:T(4,128)(2,1)} %param.35) | copy-start | bytes 49156
  7.3 16.3 %copy-start.16 = (f32[4]{0:T(128)S(1)}, f32[4]{0:T(128)}, u32[]{:S(2)}) copy-start(f32[4]{0:T(128)} %param.36) | copy-start | bytes 52
  7.3 51.6 %all-gather.23.cloned.1.call-start = ((), (), s32[]{:S(2)}) async-start(), calls=%async_computation.6 | async-start | bytes 2621440 | tf_op jit(solution)/shard_map/all_gather | solution.py:209
  8.1 87.9 %all-gather.25.cloned.1.call-start = ((), (), s32[]{:S(2)}) async-start(), calls=%async_computation.7 | async-start | bytes 2621440 | tf_op jit(solution)/shard_map/all_gather | solution.py:210
  8.8 124.1 %all-gather.27.cloned.1.call-start = ((), (), s32[]{:S(2)}) async-start(), calls=%async_computation.8 | async-start | bytes 2621440 | tf_op jit(solution)/shard_map/all_gather | solution.py:208
  9.4 171.6 %all-gather.13.cloned.1.call-start = ((), (), s32[]{:S(2)}) async-start(), calls=%async_computation.1 | async-start | bytes 2621440 | tf_op jit(solution)/shard_map/all_gather | solution.py:206
  10.0 196.7 %all-gather.19.cloned.1.call-start = ((), (), s32[]{:S(2)}) async-start(), calls=%async_computation.4 | async-start | bytes 2621440 | tf_op jit(solution)/shard_map/all_gather | solution.py:207
  10.5 233.2 %all-gather.17.cloned.1.call-start = ((), (), s32[]{:S(2)}) async-start(), calls=%async_computation.3 | async-start | bytes 2621440 | tf_op jit(solution)/shard_map/all_gather | solution.py:205
  11.3 262.0 %all-gather.15.cloned.1.call-start = ((), (), s32[]{:S(2)}) async-start(), calls=%async_computation.2 | async-start | bytes 1310720 | tf_op jit(solution)/shard_map/all_gather | solution.py:278
  11.3 54.2 %copy-start.13 = (pred[64,64]{1,0:T(8,128)(4,1)}, pred[64,64]{1,0:T(8,128)(4,1)S(1)}, u32[]{:S(2)}) copy-start(pred[64,64]{1,0:T(8,128)(4,1)S(1)} %iota_compare_fusion.1) | copy-start | bytes 12292
  65.5 1.3 copy-start.1
  74.3 27.2 %copy-start.3 = (f32[4,4,64,64]{3,2,1,0:T(8,128)S(1)}, f32[4,4,64,64]{3,2,1,0:T(8,128)}, u32[]{:S(2)}) copy-start(f32[4,4,64,64]{3,2,1,0:T(8,128)} %fusion.124) | copy-start | bytes 786436
  101.5 4.0 %copy-start.5 = (f32[4,64,4,128]{3,2,1,0:T(4,128)S(1)}, f32[4,64,4,128]{3,2,1,0:T(4,128)}, u32[]{:S(2)}) copy-start(f32[4,64,4,128]{3,2,1,0:T(4,128)} %reshape_reshape.3) | copy-start | bytes 1572868
  140.3 5.0 %copy-start.8 = (f32[4,64,4]{1,2,0:T(4,128)}, f32[4,64,4]{1,2,0:T(4,128)S(1)}, u32[]{:S(2)}) copy-start(f32[4,64,4]{1,2,0:T(4,128)S(1)} %copy.89) | copy-start | bytes 12292
  164.4 0.6 copy-start.15
  180.9 20.5 %copy-start.2 = (f32[4,64,4,128]{3,2,1,0:T(4,128)S(1)}, f32[4,64,4,128]{3,2,1,0:T(4,128)}, u32[]{:S(2)}) copy-start(f32[4,64,4,128]{3,2,1,0:T(4,128)} %copy-done.1) | copy-start | bytes 1572868
  184.3 118.0 %all-gather.21.cloned.1.call-start = ((), (), s32[]{:S(2)}) async-start(), calls=%async_computation.5 | async-start | bytes 1310720 | tf_op jit(solution)/shard_map/all_gather | solution.py:279
  210.0 5.4 %copy-start.7 = (f32[4,4,64,128]{3,2,1,0:T(8,128)S(1)}, f32[4,4,64,128]{3,2,1,0:T(8,128)}, u32[]{:S(2)}) copy-start(f32[4,4,64,128]{3,2,1,0:T(8,128)} %custom-call.2) | copy-start | bytes 1572868
  215.4 165.2 %reduce-scatter.2.cloned.1.call-start = ((), (), s32[]{:S(2)}) async-start(), calls=%async_computation.9 | async-start | bytes 1572864 | tf_op jit(solution)/shard_map/reduce_scatter | solution.py:309
  275.6 31.2 %copy-start.11 = (f32[8]{0:T(128)S(1)}, f32[8]{0:T(128)}, u32[]{:S(2)}) copy-start(f32[8]{0:T(128)} %param.30) | copy-start | bytes 100
  325.1 1.1 copy-start.4
  325.1 1.8 copy-start.6
  325.1 1.8 copy-start.12
Sparse Core Ops, SparseCore 0:
  8.9 11.7 all-gather.28
  22.5 36.3 all-gather.22
  60.8 35.1 all-gather.24
  97.7 35.1 all-gather.26
  134.6 35.1 all-gather.12
  171.5 35.1 all-gather.18
  208.5 35.1 all-gather.16
  245.3 27.9 all-gather.14
  274.9 27.3 all-gather.20
  328.7 51.7 reduce-scatter.1
where the time goes:
time: 389 us; the launch traced here: 387 us
  waiting for transfers between devices  204 us (52%)
  matrix products  92.1 us (24%)
  blocking collectives  33 us (8%)
  local copies, waits for them, and re-layouts  26.2 us (7%)
  other arithmetic  17.2 us (4%)
  between operations  14 us (4%)
    reduce_scatter x1, waiting for transfers between devices, on_device(): lax.psum_scatter((jnp.dot(sb_mixed, sb_out_w, preferred_element_type=jnp....  51.9 us
    all_gather x1, waiting for transfers between devices, on_device(): lax.all_gather(delta_key_w, 'fs', axis=0, tiled=True)  33.6 us
    all_gather x2, blocking collectives, carried_in(): lax.all_gather(part.astype(kind), axis)  33 us
    all_gather x1, waiting for transfers between devices, on_device(): value_block = lax.all_gather(sb_values, 'sp', axis=0, tiled=True)  26.7 us
    all_gather x1, waiting for transfers between devices, on_device(): key_block = lax.all_gather(sb_keys, 'sp', axis=0, tiled=True)  26.1 us
    all_gather x1, waiting for transfers between devices, on_device(): lax.all_gather(delta_query_w, 'fs', axis=0, tiled=True)  25.7 us
    dot_general x8, matrix products, on_device(): jnp.dot(portion, weight, preferred_element_type=jnp.float32)  23.6 us
    all_gather x1, waiting for transfers between devices, on_device(): lax.all_gather(delta_value_w, 'fs', axis=0, tiled=True)  21.7 us
  transfers between devices with their start and end apart: 10, of which 9 were waited for; matrix products, arithmetic and copies ran while one was open for 28% of the time, Pallas kernels for 0%

commit v1 on v0

--- a/solution.py
+++ b/solution.py
@@ -1,7 +1,11 @@
 import jax
 import jax.numpy as jnp
 from jax import lax
+from jax.experimental import pallas as pl
+from jax.experimental.pallas import tpu as pltpu
 from jax.sharding import PartitionSpec as P
+
+MESH = pl.DeviceIdType.MESH
 
 SB_DIM = 64
 GDN_DIM = 128
@@ -181,7 +185,7 @@
     return jnp.sum(partials * jnp.exp(beyond)[..., None], axis=0)
 
 
-def on_device(
+def on_device_split(
     hidden_in,
     sb_query_w,
     sb_key_w,
@@ -318,6 +322,432 @@
     return result.astype(jnp.bfloat16).reshape(1, result.shape[0], result.shape[1])
 
 
+def remote(src, dst, send, recv, axis, index):
+    return pltpu.make_async_remote_copy(
+        src_ref=src, dst_ref=dst, send_sem=send, recv_sem=recv,
+        device_id={axis: index}, device_id_type=MESH,
+    )
+
+
+def greet(axes):
+    barrier = pltpu.get_barrier_semaphore()
+    count = 0
+    for axis in axes:
+        size, me = lax.axis_size(axis), lax.axis_index(axis)
+        for k in range(1, size):
+            pl.semaphore_signal(
+                barrier, inc=1, device_id={axis: lax.rem(me + k, size)}, device_id_type=MESH
+            )
+            count += 1
+    pl.semaphore_wait(barrier, count)
+
+
+def project_kernel(
+    x_ref, w0, w1, w2, w3, w4, w5, gates_ref, shift_ref,
+    p_ref, pre_ref, shifts_ref,
+    xs, ws, x_send, x_recv, f_send, f_recv, w_send, w_recv, s_send, s_recv, l_sem, lw_sem,
+):
+    weights = (w0, w1, w2, w3, w4, w5)
+    sp, fs, tp = lax.axis_size("sp"), lax.axis_size("fs"), lax.axis_size("tp")
+    z, f, t = lax.axis_index("sp"), lax.axis_index("fs"), lax.axis_index("tp")
+    rows, half = x_ref.shape
+    depth = w0.shape[0]
+    cols = ws.shape[1] // len(weights)
+    own_x = pltpu.make_async_copy(
+        x_ref, xs.at[z, :, pl.ds(pl.multiple_of(t * half, half), half)], l_sem.at[0]
+    )
+    own_x.start()
+    own_shift = pltpu.make_async_copy(shift_ref, shifts_ref.at[z], l_sem.at[1])
+    own_shift.start()
+
+    def w_src(i, who):
+        return weights[i].at[:, pl.ds(pl.multiple_of(who * cols, cols), cols)]
+
+    def w_dst(i):
+        return ws.at[pl.ds(pl.multiple_of(f * depth, depth), depth), pl.ds(i * cols, cols)]
+
+    own_w = [
+        pltpu.make_async_copy(w_src(i, z), w_dst(i), lw_sem.at[i]) for i in range(len(weights))
+    ]
+    for c in own_w:
+        c.start()
+    greet(("sp", "fs", "tp"))
+    slot = pl.ds(pl.multiple_of(t * half, half), half)
+    w_copies, x_copies, s_copies, f_copies = [], [], [], []
+    for k in range(1, sp):
+        c = remote(
+            x_ref, xs.at[z, :, slot], x_send.at[k], x_recv.at[k], "sp", lax.rem(z + k, sp)
+        )
+        c.start()
+        x_copies.append(c)
+    for k in range(1, fs):
+        for i in range(len(weights)):
+            c = remote(
+                w_src(i, z), w_dst(i), w_send.at[k, i], w_recv.at[k, i],
+                "fs", lax.rem(f + k, fs),
+            )
+            c.start()
+            w_copies.append(c)
+    for k in range(1, sp):
+        c = remote(
+            shift_ref, shifts_ref.at[z], s_send.at[k], s_recv.at[k], "sp", lax.rem(z + k, sp)
+        )
+        c.start()
+        s_copies.append(c)
+    for k in range(sp):
+        who = lax.rem(z - k + sp, sp)
+        if k > 0:
+            x_copies[k - 1].wait_recv()
+        c = remote(
+            x_ref if k == 0 else xs.at[who, :, slot], xs.at[who, :, slot],
+            f_send.at[k], f_recv.at[k], "tp", lax.rem(t + 1, tp),
+        )
+        c.start()
+        f_copies.append(c)
+    own_x.wait()
+    own_shift.wait()
+    for c in own_w:
+        c.wait()
+    for c in w_copies:
+        c.wait_recv()
+    for k in range(sp):
+        who = lax.rem(z - k + sp, sp)
+        f_copies[k].wait_recv()
+        at = pl.ds(pl.multiple_of(who * rows, rows), rows)
+        for i in range(0, len(weights), 2):
+            out = jnp.dot(
+                xs[who], ws[:, i * cols : (i + 2) * cols], preferred_element_type=jnp.float32
+            ).astype(jnp.bfloat16)
+            p_ref[i, at, :] = out[:, :cols]
+            p_ref[i + 1, at, :] = out[:, cols:]
+        pre_ref[at, :] = jnp.dot(
+            xs[who], gates_ref[...], preferred_element_type=jnp.float32
+        )
+    for c in s_copies:
+        c.wait_recv()
+    for c in x_copies + w_copies + s_copies + f_copies:
+        c.wait_send()
+
+
+def stick_kernel(offset_ref, p_ref, out_ref):
+    rows = out_ref.shape[0]
+    i = pl.program_id(0)
+    lane = lax.broadcasted_iota(jnp.int32, (rows, out_ref.shape[1]), 1)
+    heads = offset_ref.shape[0]
+    size = out_ref.shape[1] // heads
+    below = lax.broadcasted_iota(jnp.int32, (rows, rows), 0)
+    across = lax.broadcasted_iota(jnp.int32, (rows, rows), 1)
+    after = jnp.where(below >= across, 1.0, 0.0).astype(jnp.bfloat16)
+    scale = size ** (-0.5)
+    q = p_ref[0, pl.ds(pl.multiple_of(i * rows, rows), rows), :]
+    queries = [
+        jnp.where(lane // size == h, q, jnp.zeros_like(q)) for h in range(heads)
+    ]
+
+    def block(j, carry, masked):
+        at = pl.ds(pl.multiple_of(j * rows, rows), rows)
+        keys, values = p_ref[1, at, :], p_ref[2, at, :]
+        new = []
+        for h in range(heads):
+            acc, later = carry[h]
+            score = (
+                lax.dot_general(
+                    queries[h], keys, (((1,), (1,)), ((), ())),
+                    preferred_element_type=jnp.float32,
+                ) * scale + offset_ref[h]
+            )
+            skip = -(jnp.maximum(score, 0.0) + jnp.log(1.0 + jnp.exp(-jnp.abs(score))))
+            if masked:
+                skip = jnp.where(across < below, skip, 0.0)
+            high = skip.astype(jnp.bfloat16)
+            low = (skip - high.astype(jnp.float32)).astype(jnp.bfloat16)
+            total = jnp.dot(high, after, preferred_element_type=jnp.float32) + jnp.dot(
+                low, after, preferred_element_type=jnp.float32
+            )
+            weight = jnp.exp(score + total)
+            if masked:
+                weight = jnp.where(across < below, weight, 0.0)
+            part = jnp.dot(
+                weight.astype(jnp.bfloat16), values, preferred_element_type=jnp.float32
+            )
+            new.append((acc + part * jnp.exp(later), later + total[:, :1]))
+        return tuple(new)
+
+    start = tuple(
+        (jnp.zeros(out_ref.shape, jnp.float32), jnp.zeros((rows, 1), jnp.float32))
+        for h in range(heads)
+    )
+    carry = block(i, start, True)
+    carry = lax.fori_loop(0, i, lambda n, c: block(i - 1 - n, c, False), carry)
+    mixed = carry[0][0]
+    for h in range(1, heads):
+        mixed = jnp.where(lane // size == h, carry[h][0], mixed)
+    out_ref[...] = mixed.astype(out_ref.dtype)
+
+
+def halves(a):
+    high = a.astype(jnp.bfloat16)
+    return high, (a - high.astype(jnp.float32)).astype(jnp.bfloat16)
+
+
+def product(a, b, dims=((1,), (0,))):
+    def one(x, y):
+        return lax.dot_general(x, y, (dims, ((), ())), preferred_element_type=jnp.float32)
+
+    return one(a[0], b[0]) + (one(a[0], b[1]) + one(a[1], b[0]))
+
+
+def delta_kernel(p_ref, decay_ref, strength_ref, gain_ref, out_ref, maps, adds):
+    length, size = out_ref.shape
+    span = BLOCK
+    group = 4
+    row = lax.broadcasted_iota(jnp.int32, (span, span), 0)
+    col = lax.broadcasted_iota(jnp.int32, (span, span), 1)
+    inclusive, strictly = col <= row, col < row
+    lower = jnp.where(inclusive, 1.0, 0.0)
+    unit = jnp.where(col == row, 1.0, 0.0)
+    diagonal = lax.broadcasted_iota(jnp.int32, (size, size), 0) == lax.broadcasted_iota(
+        jnp.int32, (size, size), 1
+    )
+
+    def silu(a):
+        a = a.astype(jnp.float32)
+        return a * (1.0 / (1.0 + jnp.exp(-a)))
+
+    def unit_of(a):
+        return a * lax.rsqrt(jnp.sum(a * a, axis=-1, keepdims=True) + NORM_EPS)
+
+    def prepare(step, carry):
+        blocks = []
+        for b in range(group):
+            at = pl.ds(pl.multiple_of((step * group + b) * span, span), span)
+            q = unit_of(silu(p_ref[3, at, :])) * size ** (-0.5)
+            k = unit_of(silu(p_ref[4, at, :]))
+            v = silu(p_ref[5, at, :])
+            decay = jnp.broadcast_to(decay_ref[at, :], (span, size))
+            strength = strength_ref[at, :]
+            cumulative = jnp.dot(lower, decay, precision=EXACT_MATMUL)
+            narrow = cumulative[:, :span]
+            spread = narrow - narrow.T
+            table = jnp.where(inclusive, jnp.exp(jnp.where(inclusive, spread, 0.0)), 0.0)
+            growth = jnp.exp(cumulative)
+            last = cumulative[span - 1 : span, :]
+            beta = k * strength
+            ks = halves(k)
+            near = product(halves(beta), ks, ((1,), (1,)))
+            strict = jnp.where(strictly, near * table, 0.0)
+            inside = product(halves(q), ks, ((1,), (1,))) * table
+            right = jnp.concatenate([v * strength, beta * growth], axis=1)
+            damped = k * jnp.exp(last - cumulative)
+            blocks.append([strict, inside, right, damped, q * growth, jnp.exp(last)])
+        inverses = [unit - b[0] for b in blocks]
+        powers = [halves(b[0]) for b in blocks]
+        for level in range(max(1, (span - 1).bit_length()) - 1):
+            powers = [halves(product(a, a)) for a in powers]
+            inverses = [a + product(halves(a), c) for a, c in zip(inverses, powers)]
+        for b in range(group):
+            strict, inside, right, damped, boosted, keep = blocks[b]
+            solved = halves(product(halves(inverses[b]), halves(right)))
+            state = product(halves(damped), solved, ((0,), (0,)))
+            seen = product(halves(inside), solved)
+            step_map = jnp.where(diagonal, keep, 0.0) - state[:, size:]
+            high, low = halves(step_map)
+            qhigh, qlow = halves(boosted - seen[:, size:])
+            n = step * group + b
+            maps[n, 0, :size, :] = high
+            maps[n, 0, size:, :] = qhigh
+            maps[n, 1, :size, :] = low
+            maps[n, 1, size:, :] = qlow
+            adds[n, :size, :] = state[:, :size]
+            adds[n, size:, :] = seen[:, :size]
+        return carry
+
+    lax.fori_loop(0, length // (span * group), prepare, 0)
+
+    def walk(n, memory):
+        new = product((maps[n, 0], maps[n, 1]), halves(memory)) + adds[n]
+        made = new[size:]
+        made = made * lax.rsqrt(jnp.mean(made * made, axis=-1, keepdims=True) + NORM_EPS)
+        at = pl.ds(pl.multiple_of(n * span, span), span)
+        out_ref[at, :] = (made * gain_ref[...]).astype(out_ref.dtype)
+        return new[:size]
+
+    lax.fori_loop(0, length // span, walk, jnp.zeros((size, size), jnp.float32))
+
+
+def output_kernel(
+    stick_ref, delta_ref, sw_ref, dw_ref, out_ref,
+    sticks, deltas, outgoing, incoming, own,
+    a_send, a_recv, l_sem, c_send, c_recv,
+):
+    sp, tp = lax.axis_size("sp"), lax.axis_size("tp")
+    z, t = lax.axis_index("sp"), lax.axis_index("tp")
+    rows = sticks.shape[0]
+    half = rows // tp
+    pieces = ((stick_ref, sticks), (delta_ref, deltas))
+
+    def source(ref, who):
+        return ref.at[pl.ds(pl.multiple_of(who * rows, rows), rows), :]
+
+    def slot(ref):
+        cols = stick_ref.shape[1]
+        return ref.at[:, pl.ds(pl.multiple_of(z * cols, cols), cols)]
+
+    local = [
+        pltpu.make_async_copy(source(a, z), slot(b), l_sem.at[i])
+        for i, (a, b) in enumerate(pieces)
+    ]
+    for c in local:
+        c.start()
+    greet(("sp", "tp"))
+    copies = []
+    for k in range(1, sp):
+        who = lax.rem(z + k, sp)
+        for i, (a, b) in enumerate(pieces):
+            c = remote(source(a, who), slot(b), a_send.at[k, i], a_recv.at[k, i], "sp", who)
+            c.start()
+            copies.append(c)
+    for c in local:
+        c.wait()
+    for c in copies:
+        c.wait_recv()
+    chunks, width = outgoing.shape[0], outgoing.shape[2]
+    mine = pl.ds(pl.multiple_of(t * half, half), half)
+    partner = lax.rem(t + 1, tp)
+    theirs = pl.ds(pl.multiple_of(partner * half, half), half)
+    sends = []
+    for c in range(chunks):
+        columns = slice(c * width, (c + 1) * width)
+        for which, target in ((theirs, outgoing), (mine, own)):
+            target[c] = (
+                jnp.dot(sticks[which, :], sw_ref[:, columns], preferred_element_type=jnp.float32)
+                + jnp.dot(
+                    deltas[which, :], dw_ref[:, columns], preferred_element_type=jnp.float32
+                )
+            ).astype(jnp.bfloat16)
+        sends.append(
+            remote(
+                outgoing.at[c], incoming.at[c], c_send.at[c], c_recv.at[c], "tp", partner
+            )
+        )
+        if c > 0:
+            sends[c - 1].start()
+    for c in copies:
+        c.wait_send()
+    sends[chunks - 1].start()
+    for c in range(chunks):
+        sends[c].wait_recv()
+        out_ref[:, c * width : (c + 1) * width] = (
+            own[c].astype(jnp.float32) + incoming[c].astype(jnp.float32)
+        ).astype(out_ref.dtype)
+    for c in sends:
+        c.wait_send()
+
+
+ANYWHERE = pl.BlockSpec(memory_space=pl.ANY)
+ON_CORE = pl.BlockSpec(memory_space=pltpu.VMEM)
+
+
+def on_device_heads(
+    hidden_in, sb_query_w, sb_key_w, sb_value_w, sb_offset,
+    delta_query_w, delta_key_w, delta_value_w, decay_w, write_w, write_bias,
+    decay_log_scale, decay_shift, head_gain, sb_out_w, delta_out_w,
+):
+    sp, fs, tp = lax.axis_size("sp"), lax.axis_size("fs"), lax.axis_size("tp")
+    z = lax.axis_index("sp")
+    rows, half = hidden_in.shape[1:]
+    width = half * tp
+    length = rows * sp
+    heads = decay_log_scale.shape[0]
+    sb_heads = sb_offset.shape[0] // sp
+    cols = sb_query_w.shape[1] // sp
+    gates = jnp.concatenate([decay_w, write_w], axis=1)
+    dma = pltpu.SemaphoreType.DMA
+    projected, pre, shifts = pl.pallas_call(
+        project_kernel,
+        name="project",
+        out_shape=(
+            jax.ShapeDtypeStruct((6, length, cols), jnp.bfloat16),
+            jax.ShapeDtypeStruct((length, 2 * heads), jnp.float32),
+            jax.ShapeDtypeStruct((sp, heads, rows), jnp.float32),
+        ),
+        in_specs=[ANYWHERE] * 7 + [ON_CORE, ANYWHERE],
+        out_specs=(ON_CORE, ON_CORE, ON_CORE),
+        scratch_shapes=[
+            pltpu.VMEM((sp, rows, width), jnp.bfloat16),
+            pltpu.VMEM((width, 6 * cols), jnp.bfloat16),
+            dma((sp,)), dma((sp,)), dma((sp,)), dma((sp,)),
+            dma((fs, 6)), dma((fs, 6)), dma((sp,)), dma((sp,)), dma((2,)), dma((6,)),
+        ],
+        compiler_params=pltpu.CompilerParams(
+            collective_id=0, has_side_effects=True, vmem_limit_bytes=40 * 2**20
+        ),
+    )(
+        hidden_in.reshape(rows, half), sb_query_w, sb_key_w, sb_value_w,
+        delta_query_w, delta_key_w, delta_value_w, gates, decay_shift.reshape(heads, rows),
+    )
+
+    def pick(a, start, count, axis):
+        return lax.dynamic_slice_in_dim(a, start, count, axis)
+
+    decay = (
+        -jnp.exp(pick(decay_log_scale, z, 1, 0)) * jax.nn.softplus(pick(pre, z, 1, 1))
+        + pick(shifts, z, 1, 1).reshape(length, 1)
+    )
+    strength = jax.nn.sigmoid(pick(pre, heads + z, 1, 1) + pick(write_bias, z, 1, 0))
+    stick = pl.pallas_call(
+        stick_kernel,
+        name="stick",
+        grid=(sp,),
+        out_shape=jax.ShapeDtypeStruct((length, cols), jnp.bfloat16),
+        in_specs=[
+            pl.BlockSpec(memory_space=pltpu.SMEM),
+            pl.BlockSpec((3, length, cols), lambda i: (0, 0, 0)),
+        ],
+        out_specs=pl.BlockSpec((rows, cols), lambda i: (i, 0)),
+        compiler_params=pltpu.CompilerParams(vmem_limit_bytes=40 * 2**20),
+    )(pick(sb_offset, z * sb_heads, sb_heads, 0), projected)
+    delta = pl.pallas_call(
+        delta_kernel,
+        name="delta",
+        out_shape=jax.ShapeDtypeStruct((length, cols), jnp.bfloat16),
+        in_specs=[ON_CORE] * 4,
+        out_specs=ON_CORE,
+        scratch_shapes=[
+            pltpu.VMEM((length // BLOCK, 2, cols + BLOCK, cols), jnp.bfloat16),
+            pltpu.VMEM((length // BLOCK, cols + BLOCK, cols), jnp.float32),
+        ],
+        compiler_params=pltpu.CompilerParams(vmem_limit_bytes=40 * 2**20),
+    )(projected, decay, strength, head_gain.reshape(1, -1))
+    chunks = 4
+    result = pl.pallas_call(
+        output_kernel,
+        name="output",
+        out_shape=jax.ShapeDtypeStruct((rows // tp, width), jnp.bfloat16),
+        in_specs=[ANYWHERE, ANYWHERE, ON_CORE, ON_CORE],
+        out_specs=ON_CORE,
+        scratch_shapes=[
+            pltpu.VMEM((rows, cols * sp), jnp.bfloat16),
+            pltpu.VMEM((rows, cols * sp), jnp.bfloat16),
+            pltpu.VMEM((chunks, rows // tp, width // chunks), jnp.bfloat16),
+            pltpu.VMEM((chunks, rows // tp, width // chunks), jnp.bfloat16),
+            pltpu.VMEM((chunks, rows // tp, width // chunks), jnp.bfloat16),
+            dma((sp, 2)), dma((sp, 2)), dma((2,)), dma((chunks,)), dma((chunks,)),
+        ],
+        compiler_params=pltpu.CompilerParams(
+            collective_id=1, has_side_effects=True, vmem_limit_bytes=40 * 2**20
+        ),
+    )(stick, delta, sb_out_w, delta_out_w)
+    return result.reshape(1, rows // tp, width)
+
+
+def on_device(*inputs):
+    delta_heads = inputs[11].shape[0]
+    if delta_heads == lax.axis_size("sp") and inputs[4].shape[0] % delta_heads == 0:
+        return on_device_heads(*inputs)
+    return on_device_split(*inputs)
+
+
 def solution(mesh):
     return jax.shard_map(
         on_device,

time: 389 us -> 116 us (0.30)
  waiting for transfers between devices: 204 us -> 0 us
  Pallas kernels: 0 us -> 99 us
  matrix products: 92.1 us -> 0 us
  blocking collectives: 33 us -> 0 us
  other arithmetic: 17.2 us -> 1.9 us
  between operations: 14 us -> 0.84 us
  local copies, waits for them, and re-layouts: 26.2 us -> 13.7 us
    all_gather x9 -> x0, waiting for transfers between devices: 148 us -> none  [the longest x1 33.6 us: on_device(): lax.all_gather(delta_key_w, 'fs', axis=0, tiled=True)]
    pallas_call x0 -> x4, Pallas kernels: none -> 99 us  [the longest x1 53.2 us: on_device_heads(): pl.pallas_call(project_kernel, name='project', out_shape=(jax.ShapeDtypeS...]
    dot_general x62 -> x0, matrix products: 92.1 us -> none  [the longest x8 23.6 us: on_device(): jnp.dot(portion, weight, preferred_element_type=jnp.float32)]
    reduce_scatter x1 -> x0, waiting for transfers between devices: 51.9 us -> none  [on_device(): lax.psum_scatter((jnp.dot(sb_mixed, sb_out_w, preferred_element_type=jnp....]
    all_gather x2 -> x0, blocking collectives: 33 us -> none  [carried_in(): lax.all_gather(part.astype(kind), axis)]
    mul x12 -> x0, local copies, waits for them, and re-layouts: 6.92 us -> none  [the longest x2 3.21 us: unit_rows(): vectors * vectors]
    another operation x5 -> x0, other arithmetic: 6.37 us -> none
    unnamed x40 -> x29, local copies, waits for them, and re-layouts: 5.82 us -> 12 us
  transfers between devices with their start and end apart: 10 -> 0, of which waited for: 9 -> 0; matrix products, arithmetic and copies ran while one was open for 28% -> 0% of each run, Pallas kernels for 0% -> 0%
where the time goes in v1:
time: 116 us; the launch traced here: 115 us
  Pallas kernels  99 us (85%)
  local copies, waits for them, and re-layouts  13.7 us (12%)
  other arithmetic  1.9 us (2%)
    pallas_call x1, Pallas kernels, on_device_heads(): pl.pallas_call(project_kernel, name='project', out_shape=(jax.ShapeDtypeS...  53.2 us
    pallas_call x1, Pallas kernels, on_device_heads(): pl.pallas_call(output_kernel, name='output', out_shape=jax.ShapeDtypeStru...  19 us
    pallas_call x1, Pallas kernels, on_device_heads(): pl.pallas_call(delta_kernel, name='delta', out_shape=jax.ShapeDtypeStruct...  15.2 us
    unnamed x29, local copies, waits for them, and re-layouts  12 us
    pallas_call x1, Pallas kernels, on_device_heads(): pl.pallas_call(stick_kernel, name='stick', grid=(sp,), out_shape=jax.Shap...  11.6 us

profile of v1, /device:TPU:0, one launch (start us, length us, event | category | flops | bytes accessed | tf_op | source)
XLA Modules:
  0.0 115.5 jit_solution(327481307316717441)
XLA Ops:
  0.0 0.8 pad_maximum_fusion
  0.8 0.3 copy.24.gates_ref
  1.0 0.0 copy-start.2
  1.0 1.0 copy-done.2
  2.1 0.0 copy-start.3
  2.1 1.0 copy-done.3
  3.1 0.0 copy-start.4
  3.1 1.0 copy-done.4
  4.2 1.0 copy-done.5
  5.2 1.0 copy-done.6
  6.3 1.0 copy-done.7
  7.3 1.0 copy-done.8
  8.3 0.7 copy-done.9
  9.0 53.2 %project.1 = (bf16[6,1024,128]{2,1,0:T(8,128)(2,1)S(1)}, f32[1024,8]{1,0:T(8,128)S(1)}, f32[4,4,256]{2,1,0:T(4,128)S(1)}) custom-call(bf16[256,1024]{1,0:T(8,128)(2,1)S(1)} %bitcast.8, bf16[512,512]{1,0:T(8,128)(2,1)S(1)} %copy-done.3, bf16[512,512]{1,0:T(8,128)(2,1)S(1)} %copy-done.4, bf16[512,512]{1,0:T(8,128)(2,1)S(1)} %copy-done.5, ...), custom_call_target="tpu_custom_call" | custom-call | tf_op jit(solution)/shard_map/project/pallas_call | solution.py:666
  62.2 0.0 copy-start.10
  62.3 0.2 copy.26
  62.5 0.0 copy-done.11
  62.5 0.6 dynamic_slice.19
  63.8 0.0 copy-done.12
  63.8 0.6 dynamic_slice.23
  64.4 1.1 add_divide_fusion
  65.5 0.0 copy-start.13
  65.5 0.0 copy-done.10
  65.5 15.2 %delta.1.delta_ref = bf16[1024,128]{1,0:T(8,128)(2,1)S(1)} custom-call(bf16[6,1024,128]{2,1,0:T(8,128)(2,1)S(1)} %get-tuple-element.8.p_ref, f32[1024,1]{1,0:T(8,128)S(1)} %get-tuple-element.12.decay_ref, f32[1024,1]{1,0:T(8,128)S(1)} %get-tuple-element.11.strength_ref, f32[1,128]{1,0:T(1,128)S(1)} %bitcast.10), custom_call_target="tpu_custom_call" | custom-call | tf_op jit(solution)/shard_map/delta/pallas_call | solution.py:710
  80.8 0.0 copy-done.13
  80.8 0.1 dynamic_slice.18.offset_ref
  80.8 11.6 %stick.1.stick_ref = bf16[1024,128]{1,0:T(8,128)(2,1)S(1)} custom-call(f32[2]{0:T(128)S(1)} %dynamic_slice.18.offset_ref, bf16[6,1024,128]{2,1,0:T(8,128)(2,1)S(1)} %get-tuple-element.8.p_ref), custom_call_target="tpu_custom_call" | custom-call | tf_op jit(solution)/shard_map/stick/pallas_call | solution.py:698
  92.4 0.0 copy-start
  92.5 1.6 %copy-done = bf16[512,2048]{1,0:T(8,128)(2,1)S(1)} copy-done((bf16[512,2048]{1,0:T(8,128)(2,1)S(1)}, bf16[512,2048]{1,0:T(8,128)(2,1)}, u32[]{:S(2)}) %copy-start) | copy-done | bytes 2097176
  94.0 1.6 %copy-done.1 = bf16[512,2048]{1,0:T(8,128)(2,1)S(1)} copy-done((bf16[512,2048]{1,0:T(8,128)(2,1)S(1)}, bf16[512,2048]{1,0:T(8,128)(2,1)}, u32[]{:S(2)}) %copy-start.1) | copy-done | bytes 2097176
  95.6 19.0 %output.1 = bf16[128,2048]{1,0:T(8,128)(2,1)S(1)} custom-call(bf16[1024,128]{1,0:T(8,128)(2,1)S(1)} %stick.1.stick_ref, bf16[1024,128]{1,0:T(8,128)(2,1)S(1)} %delta.1.delta_ref, bf16[512,2048]{1,0:T(8,128)(2,1)S(1)} %copy-done, bf16[512,2048]{1,0:T(8,128)(2,1)S(1)} %copy-done.1), custom_call_target="tpu_custom_call" | custom-call | tf_op jit(solution)/shard_map/output/pallas_call | solution.py:723
  114.7 0.8 copy.30
  (9 shorter events, 0.0 us)
Async XLA Ops:
  1.0 1.0 copy-start.2
  2.1 1.0 copy-start.3
  3.1 1.0 copy-start.4
  4.2 1.0 copy-start.5
  5.2 1.0 copy-start.6
  6.3 1.0 copy-start.7
  7.3 1.0 copy-start.8
  8.3 0.7 copy-start.9
  9.0 53.5 %copy-start.11 = (f32[4]{0:T(128)S(1)}, f32[4]{0:T(128)}, u32[]{:S(2)}) copy-start(f32[4]{0:T(128)} %param.27) | copy-start | bytes 52
  9.0 54.7 %copy-start.12 = (f32[4]{0:T(128)S(1)}, f32[4]{0:T(128)}, u32[]{:S(2)}) copy-start(f32[4]{0:T(128)} %param.26) | copy-start | bytes 52
  62.2 3.3 %copy-start.10 = (f32[128]{0:T(128)S(1)}, f32[128]{0:T(128)}, u32[]{:S(2)}) copy-start(f32[128]{0:T(128)} %param.29) | copy-start | bytes 1540
  65.5 15.2 %copy-start.13 = (f32[8]{0:T(128)S(1)}, f32[8]{0:T(128)}, u32[]{:S(2)}) copy-start(f32[8]{0:T(128)} %param.20) | copy-start | bytes 100
  92.4 1.6 %copy-start = (bf16[512,2048]{1,0:T(8,128)(2,1)S(1)}, bf16[512,2048]{1,0:T(8,128)(2,1)}, u32[]{:S(2)}) copy-start(bf16[512,2048]{1,0:T(8,128)(2,1)} %sw_ref.1) | copy-start | bytes 6291460
  94.0 1.6 %copy-start.1 = (bf16[512,2048]{1,0:T(8,128)(2,1)S(1)}, bf16[512,2048]{1,0:T(8,128)(2,1)}, u32[]{:S(2)}) copy-start(bf16[512,2048]{1,0:T(8,128)(2,1)} %dw_ref.1) | copy-start | bytes 6291460

commit v2 on v1

--- a/solution.py
+++ b/solution.py
@@ -6,6 +6,7 @@
 from jax.sharding import PartitionSpec as P
 
 MESH = pl.DeviceIdType.MESH
+ALL_VMEM = 67043328
 
 SB_DIM = 64
 GDN_DIM = 128
@@ -343,90 +344,174 @@
 
 
 def project_kernel(
-    x_ref, w0, w1, w2, w3, w4, w5, gates_ref, shift_ref,
-    p_ref, pre_ref, shifts_ref,
-    xs, ws, x_send, x_recv, f_send, f_recv, w_send, w_recv, s_send, s_recv, l_sem, lw_sem,
+    x_ref, w0, w1, w2, w3, w4, w5, decay_w_ref, write_w_ref, shift_ref,
+    p_ref, decay_pre_ref, write_pre_ref, shifts_ref,
+    xs, ws, decay_w, write_w,
+    x_send, x_recv, f_send, f_recv, w_send, w_recv, s_send, s_recv, l_sem, lw_sem,
 ):
     weights = (w0, w1, w2, w3, w4, w5)
-    sp, fs, tp = lax.axis_size("sp"), lax.axis_size("fs"), lax.axis_size("tp")
+    sp, tp = lax.axis_size("sp"), lax.axis_size("tp")
     z, f, t = lax.axis_index("sp"), lax.axis_index("fs"), lax.axis_index("tp")
     rows, half = x_ref.shape
     depth = w0.shape[0]
     cols = ws.shape[1] // len(weights)
-    own_x = pltpu.make_async_copy(
-        x_ref, xs.at[z, :, pl.ds(pl.multiple_of(t * half, half), half)], l_sem.at[0]
-    )
-    own_x.start()
-    own_shift = pltpu.make_async_copy(shift_ref, shifts_ref.at[z], l_sem.at[1])
-    own_shift.start()
-
-    def w_src(i, who):
-        return weights[i].at[:, pl.ds(pl.multiple_of(who * cols, cols), cols)]
-
-    def w_dst(i):
-        return ws.at[pl.ds(pl.multiple_of(f * depth, depth), depth), pl.ds(i * cols, cols)]
-
-    own_w = [
-        pltpu.make_async_copy(w_src(i, z), w_dst(i), lw_sem.at[i]) for i in range(len(weights))
+    parts = x_send.shape[2]
+    slot = pl.ds(pl.multiple_of(t * half, half), half)
+    local = [
+        pltpu.make_async_copy(x_ref, xs.at[z, :, slot], l_sem.at[0]),
+        pltpu.make_async_copy(shift_ref, shifts_ref.at[z], l_sem.at[1]),
+        pltpu.make_async_copy(decay_w_ref, decay_w, l_sem.at[2]),
+        pltpu.make_async_copy(write_w_ref, write_w, l_sem.at[3]),
     ]
-    for c in own_w:
+
+    def w_src(i):
+        return weights[i].at[:, pl.ds(pl.multiple_of(z * cols, cols), cols)]
+
+    def w_at(i, who):
+        return ws.at[pl.ds(pl.multiple_of(who * depth, depth), depth), pl.ds(i * cols, cols)]
+
+    local += [
+        pltpu.make_async_copy(w_src(i), w_at(i, f), lw_sem.at[i]) for i in range(len(weights))
+    ]
+    for c in local:
         c.start()
     greet(("sp", "fs", "tp"))
-    slot = pl.ds(pl.multiple_of(t * half, half), half)
-    w_copies, x_copies, s_copies, f_copies = [], [], [], []
-    for k in range(1, sp):
-        c = remote(
-            x_ref, xs.at[z, :, slot], x_send.at[k], x_recv.at[k], "sp", lax.rem(z + k, sp)
-        )
-        c.start()
-        x_copies.append(c)
-    for k in range(1, fs):
-        for i in range(len(weights)):
+
+    near = (f + 1 - 2 * (f % 2), f + 2 - 4 * (f // 2))
+    count = len(weights)
+    orders = (tuple(range(count)), tuple(range(count // 2, count)) + tuple(range(count // 2)))
+
+    def x_copy(way, step, part):
+        block = z - (step - 1) if way == 0 else z + (step - 1)
+        piece = pl.ds(part * (rows // parts), rows // parts)
+        there = xs.at[block, piece, slot]
+        return remote(
+            x_ref.at[piece, :] if step == 1 else there, there,
+            x_send.at[way, step, part], x_recv.at[way, step, part],
+            "sp", z + 1 if way == 0 else z - 1,
+        )
+
+    def onward(way):
+        return z + 1 < sp if way == 0 else z > 0
+
+    def comes(way, step):
+        return z >= step if way == 0 else z + step < sp
+
+    def sends(way, step):
+        return jnp.logical_and(onward(way), comes(way, step - 1))
+
+    def forward(way, step, part):
+        block = z - step if way == 0 else z + step
+        piece = pl.ds(part * (rows // parts), rows // parts)
+        there = xs.at[block, piece, slot]
+        return remote(
+            x_ref.at[piece, :] if step == 0 else there, there,
+            f_send.at[way, step, part], f_recv.at[way, step, part], "tp", lax.rem(t + 1, tp),
+        )
+
+    for part in range(parts):
+        for way in range(2):
+            @pl.when(onward(way))
+            def _():
+                x_copy(way, 1, part).start()
+
+    w_copies = {}
+    for order_at in range(count):
+        for side in range(2):
+            i = orders[side][order_at]
             c = remote(
-                w_src(i, z), w_dst(i), w_send.at[k, i], w_recv.at[k, i],
-                "fs", lax.rem(f + k, fs),
+                w_src(i), w_at(i, f), w_send.at[side, i], w_recv.at[side, i], "fs", near[side]
             )
             c.start()
-            w_copies.append(c)
+            w_copies[side, i] = c
+    s_copies = []
     for k in range(1, sp):
         c = remote(
             shift_ref, shifts_ref.at[z], s_send.at[k], s_recv.at[k], "sp", lax.rem(z + k, sp)
         )
         c.start()
         s_copies.append(c)
-    for k in range(sp):
-        who = lax.rem(z - k + sp, sp)
-        if k > 0:
-            x_copies[k - 1].wait_recv()
-        c = remote(
-            x_ref if k == 0 else xs.at[who, :, slot], xs.at[who, :, slot],
-            f_send.at[k], f_recv.at[k], "tp", lax.rem(t + 1, tp),
-        )
-        c.start()
-        f_copies.append(c)
-    own_x.wait()
-    own_shift.wait()
-    for c in own_w:
+    for part in range(parts):
+        forward(0, 0, part).start()
+
+    relays = []
+
+    def relay(position):
+        for side in range(2):
+            i = orders[side][position]
+            w_copies[side, i].wait_recv()
+            there = w_at(i, near[side])
+            c = remote(
+                there, there, w_send.at[2 + side, i], w_recv.at[2 + side, i],
+                "fs", near[1 - side],
+            )
+            c.start()
+            relays.append(c)
+
+    for step in range(1, sp):
+        relay(step - 1)
+        for part in range(parts):
+            for way in range(2):
+                @pl.when(comes(way, step))
+                def _():
+                    x_copy(way, step, part).wait_recv()
+                    forward(way, step, part).start()
+                    if step + 1 < sp:
+                        @pl.when(onward(way))
+                        def _():
+                            x_copy(way, step + 1, part).start()
+    for position in range(sp - 1, count // 2):
+        relay(position)
+    for c in local:
         c.wait()
-    for c in w_copies:
+    for side in range(2):
+        for position in range(count // 2, count):
+            w_copies[side, orders[side][position]].wait_recv()
+    for c in relays:
         c.wait_recv()
-    for k in range(sp):
-        who = lax.rem(z - k + sp, sp)
-        f_copies[k].wait_recv()
-        at = pl.ds(pl.multiple_of(who * rows, rows), rows)
-        for i in range(0, len(weights), 2):
+
+    def project(block):
+        at = pl.ds(pl.multiple_of(block * rows, rows), rows)
+        for i in range(0, count, 2):
             out = jnp.dot(
-                xs[who], ws[:, i * cols : (i + 2) * cols], preferred_element_type=jnp.float32
+                xs[block], ws[:, i * cols : (i + 2) * cols], preferred_element_type=jnp.float32
             ).astype(jnp.bfloat16)
             p_ref[i, at, :] = out[:, :cols]
             p_ref[i + 1, at, :] = out[:, cols:]
-        pre_ref[at, :] = jnp.dot(
-            xs[who], gates_ref[...], preferred_element_type=jnp.float32
-        )
+        decay_pre_ref[at, :] = lax.dot_general(
+            xs[block], decay_w[...], (((1,), (1,)), ((), ())),
+            preferred_element_type=jnp.float32,
+        )
+        write_pre_ref[at, :] = lax.dot_general(
+            xs[block], write_w[...], (((1,), (1,)), ((), ())),
+            preferred_element_type=jnp.float32,
+        )
+
+    for part in range(parts):
+        forward(0, 0, part).wait_recv()
+    project(z)
+    for step in range(1, sp):
+        for way in range(2):
+            @pl.when(comes(way, step))
+            def _():
+                for part in range(parts):
+                    forward(way, step, part).wait_recv()
+                project(z - step if way == 0 else z + step)
     for c in s_copies:
         c.wait_recv()
-    for c in x_copies + w_copies + s_copies + f_copies:
+    for c in list(w_copies.values()) + relays + s_copies:
         c.wait_send()
+    for part in range(parts):
+        forward(0, 0, part).wait_send()
+        for step in range(1, sp):
+            for way in range(2):
+                @pl.when(sends(way, step))
+                def _():
+                    x_copy(way, step, part).wait_send()
+
+                @pl.when(comes(way, step))
+                def _():
+                    forward(way, step, part).wait_send()
 
 
 def stick_kernel(offset_ref, p_ref, out_ref):
@@ -497,7 +582,11 @@
     return one(a[0], b[0]) + (one(a[0], b[1]) + one(a[1], b[0]))
 
 
-def delta_kernel(p_ref, decay_ref, strength_ref, gain_ref, out_ref, maps, adds):
+def delta_kernel(
+    decay_scale_ref, write_bias_ref, p_ref, decay_pre_ref, write_pre_ref, shifts_ref, gain_ref,
+    out_ref, maps, adds, decays, strengths,
+):
+    z = lax.axis_index("sp")
     length, size = out_ref.shape
     span = BLOCK
     group = 4
@@ -517,6 +606,28 @@
     def unit_of(a):
         return a * lax.rsqrt(jnp.sum(a * a, axis=-1, keepdims=True) + NORM_EPS)
 
+    heads = decay_pre_ref.shape[1]
+    rows = shifts_ref.shape[2]
+    mine = lax.broadcasted_iota(jnp.int32, (rows, heads), 1) == z
+    square = lax.broadcasted_iota(jnp.int32, (rows, rows), 0) == lax.broadcasted_iota(
+        jnp.int32, (rows, rows), 1
+    )
+    rate = jnp.exp(jnp.full((rows, 1), decay_scale_ref[z], jnp.float32))
+    for part in range(length // rows):
+        at = slice(part * rows, (part + 1) * rows)
+
+        def chosen(ref):
+            return jnp.sum(jnp.where(mine, ref[at, :], 0.0), axis=1, keepdims=True)
+
+        shift = jnp.sum(
+            jnp.where(square, shifts_ref[part, pl.ds(z, 1), :], 0.0), axis=1, keepdims=True
+        )
+        pre = chosen(decay_pre_ref)
+        soft = jnp.maximum(pre, 0.0) + jnp.log(1.0 + jnp.exp(-jnp.abs(pre)))
+        decays[at, :] = shift - rate * soft
+        write = chosen(write_pre_ref) + write_bias_ref[z]
+        strengths[at, :] = 1.0 / (1.0 + jnp.exp(-write))
+
     def prepare(step, carry):
         blocks = []
         for b in range(group):
@@ -524,8 +635,8 @@
             q = unit_of(silu(p_ref[3, at, :])) * size ** (-0.5)
             k = unit_of(silu(p_ref[4, at, :]))
             v = silu(p_ref[5, at, :])
-            decay = jnp.broadcast_to(decay_ref[at, :], (span, size))
-            strength = strength_ref[at, :]
+            decay = jnp.broadcast_to(decays[at, :], (span, size))
+            strength = strengths[at, :]
             cumulative = jnp.dot(lower, decay, precision=EXACT_MATMUL)
             narrow = cumulative[:, :span]
             spread = narrow - narrow.T
@@ -576,8 +687,8 @@
 
 
 def output_kernel(
-    stick_ref, delta_ref, sw_ref, dw_ref, out_ref,
-    sticks, deltas, outgoing, incoming, own,
+    stick_ref, delta_ref, sw_hbm, dw_hbm, out_ref,
+    sticks, deltas, sw_ref, dw_ref, outgoing, incoming, own,
     a_send, a_recv, l_sem, c_send, c_recv,
 ):
     sp, tp = lax.axis_size("sp"), lax.axis_size("tp")
@@ -596,6 +707,10 @@
     local = [
         pltpu.make_async_copy(source(a, z), slot(b), l_sem.at[i])
         for i, (a, b) in enumerate(pieces)
+    ]
+    local += [
+        pltpu.make_async_copy(sw_hbm, sw_ref, l_sem.at[2]),
+        pltpu.make_async_copy(dw_hbm, dw_ref, l_sem.at[3]),
     ]
     for c in local:
         c.start()
@@ -644,7 +759,7 @@
         c.wait_send()
 
 
-ANYWHERE = pl.BlockSpec(memory_space=pl.ANY)
+ANYWHERE = pl.BlockSpec(memory_space=pltpu.HBM)
 ON_CORE = pl.BlockSpec(memory_space=pltpu.VMEM)
 
 
@@ -661,40 +776,38 @@
     heads = decay_log_scale.shape[0]
     sb_heads = sb_offset.shape[0] // sp
     cols = sb_query_w.shape[1] // sp
-    gates = jnp.concatenate([decay_w, write_w], axis=1)
+    parts = 2
     dma = pltpu.SemaphoreType.DMA
-    projected, pre, shifts = pl.pallas_call(
+    projected, decay_pre, write_pre, shifts = pl.pallas_call(
         project_kernel,
         name="project",
         out_shape=(
             jax.ShapeDtypeStruct((6, length, cols), jnp.bfloat16),
-            jax.ShapeDtypeStruct((length, 2 * heads), jnp.float32),
+            jax.ShapeDtypeStruct((length, heads), jnp.float32),
+            jax.ShapeDtypeStruct((length, heads), jnp.float32),
             jax.ShapeDtypeStruct((sp, heads, rows), jnp.float32),
         ),
-        in_specs=[ANYWHERE] * 7 + [ON_CORE, ANYWHERE],
-        out_specs=(ON_CORE, ON_CORE, ON_CORE),
+        in_specs=[ANYWHERE] * 10,
+        out_specs=(ON_CORE,) * 4,
         scratch_shapes=[
             pltpu.VMEM((sp, rows, width), jnp.bfloat16),
             pltpu.VMEM((width, 6 * cols), jnp.bfloat16),
-            dma((sp,)), dma((sp,)), dma((sp,)), dma((sp,)),
-            dma((fs, 6)), dma((fs, 6)), dma((sp,)), dma((sp,)), dma((2,)), dma((6,)),
+            pltpu.VMEM((heads, width), jnp.bfloat16),
+            pltpu.VMEM((heads, width), jnp.bfloat16),
+            dma((2, sp, parts)), dma((2, sp, parts)), dma((2, sp, parts)), dma((2, sp, parts)),
+            dma((fs, 6)), dma((fs, 6)), dma((sp,)), dma((sp,)), dma((4,)), dma((6,)),
         ],
         compiler_params=pltpu.CompilerParams(
-            collective_id=0, has_side_effects=True, vmem_limit_bytes=40 * 2**20
+            collective_id=0, has_side_effects=True, vmem_limit_bytes=ALL_VMEM
         ),
     )(
         hidden_in.reshape(rows, half), sb_query_w, sb_key_w, sb_value_w,
-        delta_query_w, delta_key_w, delta_value_w, gates, decay_shift.reshape(heads, rows),
+        delta_query_w, delta_key_w, delta_value_w, decay_w.T, write_w.T, decay_shift.reshape(heads, rows),
     )
 
     def pick(a, start, count, axis):
         return lax.dynamic_slice_in_dim(a, start, count, axis)
 
-    decay = (
-        -jnp.exp(pick(decay_log_scale, z, 1, 0)) * jax.nn.softplus(pick(pre, z, 1, 1))
-        + pick(shifts, z, 1, 1).reshape(length, 1)
-    )
-    strength = jax.nn.sigmoid(pick(pre, heads + z, 1, 1) + pick(write_bias, z, 1, 0))
     stick = pl.pallas_call(
         stick_kernel,
         name="stick",
@@ -711,31 +824,38 @@
         delta_kernel,
         name="delta",
         out_shape=jax.ShapeDtypeStruct((length, cols), jnp.bfloat16),
-        in_specs=[ON_CORE] * 4,
+        in_specs=[pl.BlockSpec(memory_space=pltpu.SMEM)] * 2 + [ON_CORE] * 5,
         out_specs=ON_CORE,
         scratch_shapes=[
             pltpu.VMEM((length // BLOCK, 2, cols + BLOCK, cols), jnp.bfloat16),
             pltpu.VMEM((length // BLOCK, cols + BLOCK, cols), jnp.float32),
+            pltpu.VMEM((length, 1), jnp.float32),
+            pltpu.VMEM((length, 1), jnp.float32),
         ],
         compiler_params=pltpu.CompilerParams(vmem_limit_bytes=40 * 2**20),
-    )(projected, decay, strength, head_gain.reshape(1, -1))
+    )(
+        decay_log_scale, write_bias, projected, decay_pre, write_pre, shifts,
+        head_gain.reshape(1, -1),
+    )
     chunks = 4
     result = pl.pallas_call(
         output_kernel,
         name="output",
         out_shape=jax.ShapeDtypeStruct((rows // tp, width), jnp.bfloat16),
-        in_specs=[ANYWHERE, ANYWHERE, ON_CORE, ON_CORE],
+        in_specs=[ON_CORE, ON_CORE, ANYWHERE, ANYWHERE],
         out_specs=ON_CORE,
         scratch_shapes=[
             pltpu.VMEM((rows, cols * sp), jnp.bfloat16),
             pltpu.VMEM((rows, cols * sp), jnp.bfloat16),
+            pltpu.VMEM(sb_out_w.shape, jnp.bfloat16),
+            pltpu.VMEM(delta_out_w.shape, jnp.bfloat16),
             pltpu.VMEM((chunks, rows // tp, width // chunks), jnp.bfloat16),
             pltpu.VMEM((chunks, rows // tp, width // chunks), jnp.bfloat16),
             pltpu.VMEM((chunks, rows // tp, width // chunks), jnp.bfloat16),
-            dma((sp, 2)), dma((sp, 2)), dma((2,)), dma((chunks,)), dma((chunks,)),
+            dma((sp, 2)), dma((sp, 2)), dma((4,)), dma((chunks,)), dma((chunks,)),
         ],
         compiler_params=pltpu.CompilerParams(
-            collective_id=1, has_side_effects=True, vmem_limit_bytes=40 * 2**20
+            collective_id=1, has_side_effects=True, vmem_limit_bytes=ALL_VMEM
         ),
     )(stick, delta, sb_out_w, delta_out_w)
     return result.reshape(1, rows // tp, width)
@@ -743,7 +863,8 @@
 
 def on_device(*inputs):
     delta_heads = inputs[11].shape[0]
-    if delta_heads == lax.axis_size("sp") and inputs[4].shape[0] % delta_heads == 0:
+    square = lax.axis_size("fs") == 4 and lax.axis_size("tp") == 2
+    if square and delta_heads == lax.axis_size("sp") and inputs[4].shape[0] % delta_heads == 0:
         return on_device_heads(*inputs)
     return on_device_split(*inputs)
 

time: 116 us -> 104 us (0.90)
  Pallas kernels: 99 us -> 93.8 us
  local copies, waits for them, and re-layouts: 13.7 us -> 9.53 us
  other arithmetic: 1.9 us -> 0 us
    pallas_call x1, Pallas kernels: 53.2 us -> 49.3 us  [on_device_heads(): pl.pallas_call(project_kernel, name='project', out_shape=(jax.ShapeDtypeS...]
    unnamed x29 -> x23, local copies, waits for them, and re-layouts: 12 us -> 9.45 us
    pallas_call x1, Pallas kernels: 19 us -> 16.7 us  [on_device_heads(): pl.pallas_call(output_kernel, name='output', out_shape=jax.ShapeDtypeStru...]
    dynamic_slice x4 -> x1, local copies, waits for them, and re-layouts: 1.27 us -> 0.07 us  [pick(): return lax.dynamic_slice_in_dim(a, start, count, axis)]
where the time goes in v2:
time: 104 us; the launch traced here: 103 us
  Pallas kernels  93.8 us (90%)
  local copies, waits for them, and re-layouts  9.53 us (9%)
    pallas_call x1, Pallas kernels, on_device_heads(): pl.pallas_call(project_kernel, name='project', out_shape=(jax.ShapeDtypeS...  49.3 us
    pallas_call x1, Pallas kernels, on_device_heads(): pl.pallas_call(output_kernel, name='output', out_shape=jax.ShapeDtypeStru...  16.7 us
    pallas_call x1, Pallas kernels, on_device_heads(): pl.pallas_call(delta_kernel, name='delta', out_shape=jax.ShapeDtypeStruct...  16.3 us
    pallas_call x1, Pallas kernels, on_device_heads(): pl.pallas_call(stick_kernel, name='stick', grid=(sp,), out_shape=jax.Shap...  11.6 us
    unnamed x23, local copies, waits for them, and re-layouts  9.45 us

profile of v2, /device:TPU:0, one launch (start us, length us, event | category | flops | bytes accessed | tf_op | source)
XLA Modules:
  0.0 103.4 jit_solution(74752272489661245)
XLA Ops:
  0.0 49.3 %project.1 = (bf16[6,1024,128]{2,1,0:T(8,128)(2,1)}, f32[1024,4]{1,0:T(8,128)}, f32[1024,4]{1,0:T(8,128)}, f32[4,4,256]{2,1,0:T(4,128)}) custom-call(bf16[256,1024]{1,0:T(8,128)(2,1)} %bitcast.8, bf16[512,512]{1,0:T(8,128)(2,1)} %w0.1, bf16[512,512]{1,0:T(8,128)(2,1)} %w1.1, bf16[512,512]{1,0:T(8,128)(2,1)} %w2.1, bf16[512,512]{1,0:T(8,128)(2,1)} %w3.1, ...), custom_call_target="tpu_custom_call" | custom-call | tf_op jit(solution)/shard_map/project/pallas_call | solution.py:781
  49.3 0.0 copy-start.10
  49.3 0.0 copy-start
  49.3 1.4 %copy-done = bf16[6,1024,128]{2,1,0:T(8,128)(2,1)S(1)} copy-done((bf16[6,1024,128]{2,1,0:T(8,128)(2,1)S(1)}, bf16[6,1024,128]{2,1,0:T(8,128)(2,1)}, u32[]{:S(2)}) %copy-start) | copy-done | bytes 1572888
  50.7 0.0 copy-start.4
  50.7 1.0 %copy-done.4 = f32[1024,4]{1,0:T(8,128)S(1)} copy-done((f32[1024,4]{1,0:T(8,128)S(1)}, f32[1024,4]{1,0:T(8,128)}, u32[]{:S(2)}) %copy-start.4) | copy-done | bytes 16408
  51.8 0.0 copy-start.5
  51.8 1.0 %copy-done.5 = f32[1024,4]{1,0:T(8,128)S(1)} copy-done((f32[1024,4]{1,0:T(8,128)S(1)}, f32[1024,4]{1,0:T(8,128)}, u32[]{:S(2)}) %copy-start.5) | copy-done | bytes 16408
  52.8 0.0 copy-start.6
  52.8 0.7 copy-done.6
  53.5 0.0 copy-start.7
  53.5 0.7 copy-done.7
  54.2 0.0 copy-start.8
  54.2 0.7 copy-done.8
  54.8 0.0 copy-start.9
  54.8 0.7 copy-done.9
  55.5 0.0 copy-start.1
  55.5 16.3 %delta.1.delta_ref = bf16[1024,128]{1,0:T(8,128)(2,1)S(1)} custom-call(f32[4]{0:T(128)S(1)} %copy-done.7, f32[4]{0:T(128)S(1)} %copy-done.8, bf16[6,1024,128]{2,1,0:T(8,128)(2,1)S(1)} %copy-done, f32[1024,4]{1,0:T(8,128)S(1)} %copy-done.4, f32[1024,4]{1,0:T(8,128)S(1)} %copy-done.5, f32[4,4,256]{2,1,0:T(4,128)S(1)} %copy-done.6, f32[1,128]{1,0:T(1,128)S(1)} %bitcast.6), custom_call_target="tpu_custom_call" | custom-call | tf_op jit(solution)/shard_map/delta/pallas_call | solution.py:823
  71.8 0.0 copy-start.2
  71.8 0.7 copy-done.2
  72.5 0.0 copy-done.10
  72.5 0.1 dynamic_slice.3.offset_ref
  72.5 0.0 copy-done.1
  72.5 11.6 %stick.1.stick_ref = bf16[1024,128]{1,0:T(8,128)(2,1)S(1)} custom-call(f32[2]{0:T(128)S(1)} %dynamic_slice.3.offset_ref, bf16[6,1024,128]{2,1,0:T(8,128)(2,1)S(1)} %copy-done.1), custom_call_target="tpu_custom_call" | custom-call | tf_op jit(solution)/shard_map/stick/pallas_call | solution.py:811
  84.1 0.0 copy-start.3
  84.2 0.7 copy-done.3
  84.9 16.7 %output.1 = bf16[128,2048]{1,0:T(8,128)(2,1)} custom-call(bf16[1024,128]{1,0:T(8,128)(2,1)} %copy-done.3, bf16[1024,128]{1,0:T(8,128)(2,1)} %copy-done.2, bf16[512,2048]{1,0:T(8,128)(2,1)} %sw_hbm.1, bf16[512,2048]{1,0:T(8,128)(2,1)} %dw_hbm.1), custom_call_target="tpu_custom_call" | custom-call | tf_op jit(solution)/shard_map/output/pallas_call | solution.py:841
  101.6 1.9 %copy.18 = bf16[1,128,2048]{2,1,0:T(8,128)(2,1)} copy(bf16[1,128,2048]{2,1,0:T(8,128)(2,1)} %bitcast.7) | data formatting | bytes 1048576
Async XLA Ops:
  49.3 23.2 %copy-start.10 = (f32[8]{0:T(128)S(1)}, f32[8]{0:T(128)}, u32[]{:S(2)}) copy-start(f32[8]{0:T(128)} %param.20) | copy-start | bytes 100
  49.3 1.4 %copy-start = (bf16[6,1024,128]{2,1,0:T(8,128)(2,1)S(1)}, bf16[6,1024,128]{2,1,0:T(8,128)(2,1)}, u32[]{:S(2)}) copy-start(bf16[6,1024,128]{2,1,0:T(8,128)(2,1)} %get-tuple-element.9.p_ref) | copy-start | bytes 4718596
  50.7 1.0 %copy-start.4 = (f32[1024,4]{1,0:T(8,128)S(1)}, f32[1024,4]{1,0:T(8,128)}, u32[]{:S(2)}) copy-start(f32[1024,4]{1,0:T(8,128)} %get-tuple-element.10.decay_pre_ref) | copy-start | bytes 49156
  51.8 1.0 %copy-start.5 = (f32[1024,4]{1,0:T(8,128)S(1)}, f32[1024,4]{1,0:T(8,128)}, u32[]{:S(2)}) copy-start(f32[1024,4]{1,0:T(8,128)} %get-tuple-element.11.write_pre_ref) | copy-start | bytes 49156
  52.8 0.7 copy-start.6
  53.5 0.7 copy-start.7
  54.2 0.7 copy-start.8
  54.8 0.7 copy-start.9
  55.5 17.1 %copy-start.1 = (bf16[6,1024,128]{2,1,0:T(8,128)(2,1)S(1)}, bf16[6,1024,128]{2,1,0:T(8,128)(2,1)}, u32[]{:S(2)}) copy-start(bf16[6,1024,128]{2,1,0:T(8,128)(2,1)} %get-tuple-element.9.p_ref) | copy-start | bytes 4718596
  71.8 0.7 copy-start.2
  84.1 0.7 copy-start.3
